TPU v7x, 32 devices: a whole 2x2x4 slice. The times are simulated.
32 devices in a mesh: fs: 16 (over z, y, core), tp: 2 (over x).
Axes of the slice: x: 2, y: 2, z: 4, core: 2. Of those that a mesh axis runs over, the one named last changes fastest.
Arguments:
- saved_input: bfloat16 [8192, 3072], P('fs'), may hold values from -6 to 6
- output_cotangent: bfloat16 [8192, 3072], P('fs'), may hold values from -6 to 6
- recurrent_output: bfloat16 [8192, 1536], P('fs', 'tp'), may hold values from -6 to 6
- forget_logit: bfloat16 [8192, 1536], P('fs', 'tp'), may hold values from -12 to 12
- forget_cotangent: bfloat16 [8192, 1536], P('fs', 'tp'), may hold values from -6 to 6
- lower_bound: float32 [1536], P('tp'), may hold values from 0.2 to 0.9
- basis_in: bfloat16 [3072, 384], P('fs'), may hold values from -1.2629537 to 1.2629537
- basis_out: bfloat16 [3072, 384], P('fs'), may hold values from -1.2629537 to 1.2629537
- moment_in: float32 [384, 1536], P('fs', 'tp'), may hold values from -6 to 6
- second_in: float32 [384, 1536], P('fs', 'tp'), may hold values from 0.25 to 4
- moment_out: float32 [384, 1536], P('fs', 'tp'), may hold values from -6 to 6
- second_out: float32 [384, 1536], P('fs', 'tp'), may hold values from 0.25 to 4
- weight_in: float32 [3072, 1536], P('fs', 'tp'), may hold values from -0.109375 to 0.109375
- weight_out: float32 [1536, 3072], P('tp', 'fs'), may hold values from -0.15625 to 0.15625
Outputs:
- moment_in_new: float32 [384, 1536], P('fs', 'tp')
- second_in_new: float32 [384, 1536], P('fs', 'tp')
- moment_out_new: float32 [384, 1536], P('fs', 'tp')
- second_out_new: float32 [384, 1536], P('fs', 'tp')
- weight_in_new: float32 [3072, 1536], P('fs', 'tp')
- weight_out_new: float32 [1536, 3072], P('tp', 'fs')
- copy_in: bfloat16 [3072, 1536], P(None, 'tp')
- copy_out: bfloat16 [1536, 3072], P('tp')
All inputs are finite; a program needn't handle non-finite values.
Results may differ from a plain program's by a relative error of at most 0.0023.
Values may be sent and summed in bfloat16 or wider, within the bound.
A program may use at most 64 MiB of HBM per device.

v0:
```python
import jax
import jax.numpy as jnp
from jax import lax
from jax.sharding import PartitionSpec as P

HW = 1536
R = 384


def body(
    saved_input,
    output_cotangent,
    recurrent_output,
    forget_logit,
    forget_cotangent,
    lower_bound,
    basis_in,
    basis_out,
    moment_in,
    second_in,
    moment_out,
    second_out,
    weight_in,
    weight_out,
):
    sig = jax.nn.sigmoid(forget_logit.astype(jnp.float32))
    gate_cot = (
        forget_cotangent.astype(jnp.float32) * (1.0 - lower_bound)[None, :] * sig * (1.0 - sig)
    ).astype(jnp.bfloat16)
    full_in, full_out = (
        lax.all_gather(basis_in, "fs", axis=0, tiled=True),
        lax.all_gather(basis_out, "fs", axis=0, tiled=True),
    )
    coded_in = jnp.dot(saved_input, full_in, preferred_element_type=jnp.float32).astype(
        jnp.bfloat16
    )
    coded_out = jnp.dot(output_cotangent, full_out, preferred_element_type=jnp.float32).astype(
        jnp.bfloat16
    )
    units = recurrent_output.shape[1]
    contract = (((0,), (0,)), ((), ()))
    term_in = lax.dot_general(coded_in, gate_cot, contract, preferred_element_type=jnp.float32)
    term_out = lax.dot_general(
        coded_out, recurrent_output, contract, preferred_element_type=jnp.float32
    )
    lowrank = lax.psum_scatter(
        jnp.concatenate([term_in, term_out], axis=1), "fs", scatter_dimension=0, tiled=True
    )
    total = lax.psum(jnp.sum(lowrank * lowrank), ("fs", "tp"))
    clip = jnp.minimum(1.0, jnp.sqrt(jnp.float32(2 * R * HW)) * lax.rsqrt(total + 1e-06))
    grads = clip * lowrank
    moments = 0.8 * jnp.concatenate([moment_in, moment_out], axis=1) + 0.2 * grads
    seconds = 0.9 * jnp.concatenate([second_in, second_out], axis=1) + 0.1 * grads * grads
    stepping = moments / (jnp.sqrt(seconds) + 1e-08)
    whole_step = lax.all_gather(stepping, "fs", axis=0, tiled=True)
    update_in = jnp.dot(
        basis_in.astype(jnp.float32), whole_step[:, :units], precision=lax.Precision.HIGHEST
    )
    update_out = jnp.dot(
        whole_step[:, units:].T, basis_out.astype(jnp.float32).T, precision=lax.Precision.HIGHEST
    )
    weight_in_new = weight_in - 0.01 * update_in
    weight_out_new = weight_out - 0.01 * update_out
    copy_in, copy_out = (
        lax.all_gather(weight_in_new.astype(jnp.bfloat16), "fs", axis=0, tiled=True),
        lax.all_gather(weight_out_new.astype(jnp.bfloat16), "fs", axis=1, tiled=True),
    )
    return (
        moments[:, :units],
        seconds[:, :units],
        moments[:, units:],
        seconds[:, units:],
        weight_in_new,
        weight_out_new,
        copy_in,
        copy_out,
    )


def solution(mesh):
    return jax.shard_map(
        body,
        mesh=mesh,
        in_specs=(
            P("fs", None),
            P("fs", None),
            P("fs", "tp"),
            P("fs", "tp"),
            P("fs", "tp"),
            P("tp"),
            P("fs", None),
            P("fs", None),
            P("fs", "tp"),
            P("fs", "tp"),
            P("fs", "tp"),
            P("fs", "tp"),
            P("fs", "tp"),
            P("tp", "fs"),
        ),
        out_specs=(
            P("fs", "tp"),
            P("fs", "tp"),
            P("fs", "tp"),
            P("fs", "tp"),
            P("fs", "tp"),
            P("tp", "fs"),
            P(None, "tp"),
            P("tp", None),
        ),
        check_vma=False,
    )
```

profile of v0, /device:TPU:0, one launch (start us, length us, event | category | flops | bytes accessed | tf_op | source)
XLA Modules:
  0.0 377.6 jit_solution(13971637352224902390)
XLA Ops:
  7.2 0.7 all-gather.8.cloned.1.call-update
  8.0 0.7 all-gather.6.cloned.1.call-update
  8.7 0.0 reduce-scatter.2.cloned.1.call-start
  8.7 0.7 broadcast_subtract_fusion
  9.4 45.9 %all-gather.8.cloned.1.call-done = bf16[3072,384]{1,0:T(8,128)(2,1)} async-done(((bf16[192,384]{1,0:T(8,128)(2,1)}), bf16[3072,384]{1,0:T(8,128)(2,1)}) %all-gather.8.cloned.1.call-update) | async-done | bytes 2359312 | tf_op jit(solution)/shard_map/all_gather | solution.py:32
  55.3 5.2 %fusion.6 = f32[384,768]{1,0:T(8,128)} fusion(bf16[512,768]{1,0:T(8,128)(2,1)} %param.16, bf16[512,3072]{1,0:T(8,128)(2,1)S(1)} %copy-done, bf16[3072,384]{1,0:T(8,128)(2,1)} %all-gather.8.cloned.1.call-done), kind=kOutput, calls=%fused_computation.12 | convolution fusion | flops 1510146048 | bytes 7471104 | tf_op jit(solution)/shard_map/dot_general | solution.py:43
  60.5 38.1 %all-gather.6.cloned.1.call-done = bf16[3072,384]{1,0:T(8,128)(2,1)} async-done(((bf16[192,384]{1,0:T(8,128)(2,1)}), bf16[3072,384]{1,0:T(8,128)(2,1)}) %all-gather.6.cloned.1.call-update) | async-done | bytes 2359312 | tf_op jit(solution)/shard_map/all_gather | solution.py:31
  98.7 6.5 %fusion.5 = f32[384,768]{1,0:T(8,128)} fusion(bf16[512,3072]{1,0:T(8,128)(2,1)} %param.14, bf16[3072,384]{1,0:T(8,128)(2,1)} %all-gather.6.cloned.1.call-done, bf16[512,768]{1,0:T(8,128)(2,1)} %param.17, bf16[512,768]{1,0:T(8,128)(2,1)} %param.18, f32[768]{0:T(1024)S(1)} %broadcast_subtract_fusion), kind=kOutput, calls=%fused_computation.11 | convolution fusion | flops 1514078208 | bytes 8260608 | tf_op jit(solution)/shard_map/dot_general | solution.py:42
  105.2 3.3 pad_maximum_fusion
  108.5 0.0 all-gather.10.cloned.1.call-start
  108.5 62.0 %reduce-scatter.2.cloned.1.call-done = f32[24,1536]{1,0:T(8,128)} async-done(((f32[384,1536]{1,0:T(8,128)}), f32[24,1536]{1,0:T(8,128)}) %reduce-scatter.2.cloned.1.call-update) | async-done | bytes 147472 | tf_op jit(solution)/shard_map/reduce_scatter | solution.py:46
  170.6 1.6 multiply_reduce_fusion
  172.1 40.0 %psum.7 = f32[]{:T(128)} all-reduce(f32[]{:T(128)} %multiply_reduce_fusion), channel_id=1, replica_groups=mesh['fs'=16,'tp'=2] {'fs','tp'}, use_global_device_ids=true, to_apply=%region_2.0 | all-reduce | flops 1 | bytes 8 | tf_op jit(solution)/shard_map/psum | solution.py:49
  212.8 1.8 add_divide_fusion
  214.6 0.0 all-gather.14.cloned.1.call-start
  214.7 41.8 %all-gather.10.cloned.1.call-done = f32[384,1536]{1,0:T(8,128)} async-done(((f32[24,1536]{1,0:T(8,128)}), f32[384,1536]{1,0:T(8,128)}) %all-gather.10.cloned.1.call-update) | async-done | bytes 2359312 | tf_op jit(solution)/shard_map/all_gather | solution.py:55
  256.5 3.0 fusion.16
  259.5 0.0 all-gather.12.cloned.1.call-start
  259.6 3.0 fusion.15
  262.6 1.6 fusion.13
  264.3 47.2 %all-gather.14.cloned.1.call-done = bf16[768,3072]{0,1:T(8,128)(2,1)} async-done(((bf16[768,192]{0,1:T(8,128)(2,1)}), bf16[768,3072]{0,1:T(8,128)(2,1)}) %all-gather.14.cloned.1.call-update) | async-done | bytes 4718608 | tf_op jit(solution)/shard_map/all_gather | solution.py:66
  311.5 6.6 %copy.22 = bf16[768,3072]{1,0:T(8,128)(2,1)} copy(bf16[768,3072]{0,1:T(8,128)(2,1)} %all-gather.14.cloned.1.call-done) | data formatting | bytes 9437184
  318.1 47.8 %all-gather.12.cloned.1.call-done = bf16[3072,768]{1,0:T(8,128)(2,1)} async-done(((bf16[192,768]{1,0:T(8,128)(2,1)}), bf16[3072,768]{1,0:T(8,128)(2,1)}) %all-gather.12.cloned.1.call-update) | async-done | bytes 4718608 | tf_op jit(solution)/shard_map/all_gather | solution.py:65
  365.9 4.8 %copy.24 = bf16[3072,768]{1,0:T(8,128)(2,1)} copy(bf16[3072,768]{1,0:T(8,128)(2,1)} %all-gather.12.cloned.1.call-done) | data formatting | bytes 9437184
  (16 shorter events, 0.2 us)
Async XLA Ops:
  7.2 48.2 %copy-start = (bf16[512,3072]{1,0:T(8,128)(2,1)S(1)}, bf16[512,3072]{1,0:T(8,128)(2,1)}, u32[]{:S(2)}) copy-start(bf16[512,3072]{1,0:T(8,128)(2,1)} %param.15) | copy-start | bytes 9437188
  7.2 48.2 %all-gather.8.cloned.1.call-start = ((), (), s32[]{:S(2)}) async-start(), calls=%async_computation.2 | async-start | bytes 2506752 | tf_op jit(solution)/shard_map/all_gather | solution.py:32
  7.9 90.8 %all-gather.6.cloned.1.call-start = ((), (), s32[]{:S(2)}) async-start(), calls=%async_computation.1 | async-start | bytes 2506752 | tf_op jit(solution)/shard_map/all_gather | solution.py:31
  8.7 161.9 %reduce-scatter.2.cloned.1.call-start = ((), (), s32[]{:S(2)}) async-start(), calls=%async_computation.3 | async-start | bytes 2506752 | tf_op jit(solution)/shard_map/reduce_scatter | solution.py:46
  108.4 104.3 %copy-start.4 = (f32[24,768]{1,0:T(8,128)S(1)}, f32[24,768]{1,0:T(8,128)}, u32[]{:S(2)}) copy-start(f32[24,768]{1,0:T(8,128)} %param.25) | copy-start | bytes 221188
  108.5 148.0 %copy-start.1 = (bf16[192,384]{1,0:T(8,128)(2,1)S(1)}, bf16[192,384]{1,0:T(8,128)(2,1)}, u32[]{:S(2)}) copy-start(bf16[192,384]{1,0:T(8,128)(2,1)} %param.21) | copy-start | bytes 442372
  108.5 151.1 %copy-start.2 = (bf16[192,384]{1,0:T(8,128)(2,1)S(1)}, bf16[192,384]{1,0:T(8,128)(2,1)}, u32[]{:S(2)}) copy-start(bf16[192,384]{1,0:T(8,128)(2,1)} %param.20) | copy-start | bytes 442372
  108.5 148.0 %all-gather.10.cloned.1.call-start = ((), (), s32[]{:S(2)}) async-start(), calls=%async_computation.4 | async-start | bytes 2506752 | tf_op jit(solution)/shard_map/all_gather | solution.py:55
  214.6 96.9 %all-gather.14.cloned.1.call-start = ((), (), s32[]{:S(2)}) async-start(), calls=%async_computation.6 | async-start | bytes 5013504 | tf_op jit(solution)/shard_map/all_gather | solution.py:66
  259.5 3.1 copy-start.3
  259.5 106.4 %all-gather.12.cloned.1.call-start = ((), (), s32[]{:S(2)}) async-start(), calls=%async_computation.5 | async-start | bytes 5013504 | tf_op jit(solution)/shard_map/all_gather | solution.py:65
Sparse Core Ops, SparseCore 0:
  10.3 45.0 all-gather.7
  57.6 41.0 all-gather.5
  108.6 61.9 reduce-scatter.1
  214.8 41.6 all-gather.9
  259.6 51.8 all-gather.13
  314.2 51.6 all-gather.11
where the time goes:
time: 378 us
  waiting for transfers between devices  284 us (75%)
  blocking collectives  40 us (11%)
  matrix products  17.7 us (5%)
  between operations  14.9 us (4%)
  local copies, waits for them, and re-layouts  13.1 us (3%)
  other arithmetic  7.34 us (2%)
    reduce_scatter x1, waiting for transfers between devices, body(): lax.psum_scatter(jnp.concatenate([term_in, term_out], axis=1), 'fs', scat...  62 us
    all_gather x1, waiting for transfers between devices, body(): lax.all_gather(weight_in_new.astype(jnp.bfloat16), 'fs', axis=0, tiled=True)  47.8 us
    all_gather x1, waiting for transfers between devices, body(): lax.all_gather(weight_out_new.astype(jnp.bfloat16), 'fs', axis=1, tiled=T...  47.2 us
    all_gather x1, waiting for transfers between devices, body(): lax.all_gather(basis_out, 'fs', axis=0, tiled=True)  45.9 us
    all_gather x1, waiting for transfers between devices, body(): whole_step = lax.all_gather(stepping, 'fs', axis=0, tiled=True)  41.8 us
    psum x1, blocking collectives, body(): total = lax.psum(jnp.sum(lowrank * lowrank), ('fs', 'tp'))  40 us
    all_gather x1, waiting for transfers between devices, body(): lax.all_gather(basis_in, 'fs', axis=0, tiled=True)  38.1 us
    unnamed x12, local copies, waits for them, and re-layouts  11.5 us
  transfers between devices with their start and end apart: 6, of which 6 were waited for; matrix products, arithmetic and copies ran while one was open for 5% of the time, Pallas kernels for 0%

commit v1 on v0

v1 whole, which is shorter than its diff:
```python
import functools

import jax
import jax.numpy as jnp
from jax import lax
from jax.experimental import pallas as pl
from jax.experimental.pallas import tpu as pltpu
from jax.sharding import PartitionSpec as P

MESH = pl.DeviceIdType.MESH
F32 = jnp.float32
BF16 = jnp.bfloat16
UNROLL = 16


def loop(start, stop, body):
    if stop - start <= UNROLL:
        for i in range(start, stop):
            body(i)
    else:

        @pl.loop(start, stop)
        def _(i):
            body(i)


def mod(value, n):
    return lax.rem(value + 2 * n, n)


def kernel(
    nf,
    nt,
    limit,
    x_hbm,
    y_hbm,
    rec_hbm,
    logit_hbm,
    fcot_hbm,
    lower_ref,
    basis_in_hbm,
    basis_out_hbm,
    m_in,
    s_in,
    m_out,
    s_out,
    w_in,
    w_out,
    mn_in,
    sn_in,
    mn_out,
    sn_out,
    wn_in,
    wn_out,
    copy_in,
    copy_out,
    x,
    y,
    rec,
    logit,
    fcot,
    bas_in,
    bas_out,
    gate,
    term,
    coded,
    part,
    peer,
    hop,
    step,
    flat,
    wb_in,
    wb_out,
    tots,
    load_sem,
    base_sem,
    send_sem,
    ring_a,
    ring_b,
    ring_d,
    ring_f,
    pair_sem,
    tot_sem,
):
    f = lax.axis_index("fs")
    tp = lax.axis_index("tp")
    n = nf // 2
    z = n // 2
    core = lax.rem(f, 2)
    chip = f // 2
    row, column = chip // 2, lax.rem(chip, 2)
    me = (1 - column) * row + column * (n - 1 - row)
    partner = (f + 1 - 2 * core, tp)

    def chip_at(position):
        side = position // z
        return 2 * ((1 - side) * position + side * (n - 1 - position)) + side

    def dev_at(position):
        return chip_at(position) * 2 + core

    ways = (1, -1)
    ahead = tuple((dev_at(mod(me + way, n)), tp) for way in ways)

    loads = [
        pltpu.make_async_copy(src, dst, load_sem.at[i])
        for i, (src, dst) in enumerate(
            ((logit_hbm, logit), (fcot_hbm, fcot), (x_hbm, x), (y_hbm, y), (rec_hbm, rec))
        )
    ]
    depth = basis_in_hbm.shape[0]
    cut = 2 if depth % 32 == 0 else 1
    piece = depth // cut

    def rows(ref, dev, c):
        return ref.at[pl.ds(pl.multiple_of(dev * depth + c * piece, piece), piece)]

    def own(ref, dev):
        return ref.at[pl.ds(pl.multiple_of(dev * depth, depth), depth)]

    own_loads = [
        pltpu.make_async_copy(basis_in_hbm, own(bas_in, f), base_sem.at[0]),
        pltpu.make_async_copy(basis_out_hbm, own(bas_out, f), base_sem.at[1]),
    ]
    for copy in own_loads + loads:
        copy.start()

    barrier = pltpu.get_barrier_semaphore()
    everyone = nf * nt
    my_id = f * nt + tp

    def other(i):
        target = lax.rem(my_id + i, everyone)
        return (target // nt, lax.rem(target, nt))

    @pl.loop(1, everyone)
    def _(i):
        pl.semaphore_signal(barrier, inc=1, device_id=other(i), device_id_type=MESH)

    pl.semaphore_wait(barrier, everyone - 1)

    def gather(view, chunks, ring_sem, phase, between=None):
        def ring_copy(t, s, c):
            block = view(t, dev_at(mod(me - ways[t] * s, n)), c)
            return pltpu.make_async_remote_copy(
                src_ref=block,
                dst_ref=block,
                send_sem=send_sem.at[phase, t, s, c],
                recv_sem=ring_sem.at[t, s, c],
                device_id=ahead[t],
                device_id_type=MESH,
            )

        def pair_copy(t, s, c):
            block = view(t, dev_at(mod(me - ways[t] * s, n)), c)
            return pltpu.make_async_remote_copy(
                src_ref=block,
                dst_ref=block,
                send_sem=pair_sem.at[phase, 0, t, s, c],
                recv_sem=pair_sem.at[phase, 1, t, s, c],
                device_id=partner,
                device_id_type=MESH,
            )

        both = [(t, c) for c in range(chunks) for t in range(2)]

        def stage(s, first=False, last=False):
            for t, c in both:
                if not first:
                    ring_copy(t, s - 1, c).wait_recv()
                if not last:
                    ring_copy(t, s, c).start()
                pair_copy(t, s, c).start()

        stage(0, first=True)
        if between is not None:
            between()
        loop(1, n - 1, stage)
        stage(n - 1, last=True)

        def finish(s):
            for t, c in both:
                pair_copy(t, s, c).wait()

        def sent(s):
            for t, c in both:
                ring_copy(t, s, c).wait_send()

        loop(0, n, finish)
        loop(0, n - 1, sent)

    def make_gate():
        loads[0].wait()
        loads[1].wait()
        tile = 64

        @pl.loop(0, gate.shape[0] // tile)
        def _(i):
            at = pl.ds(pl.multiple_of(i * tile, tile), tile)
            sig = jax.nn.sigmoid(logit[at].astype(F32))
            gate[at] = (
                fcot[at].astype(F32) * (1.0 - lower_ref[...]) * sig * (1.0 - sig)
            ).astype(BF16)

    for copy in own_loads:
        copy.wait()
    gather(lambda t, dev, c: rows((bas_in, bas_out)[t], dev, c), cut, ring_a, 0, make_gate)

    for copy in loads[2:]:
        copy.wait()
    units = gate.shape[1]
    span = part.shape[2]
    lanes = 2 if units % 256 == 0 else 1
    width = units // lanes

    for t, (data, basis, cot) in enumerate(((x, bas_in, gate), (y, bas_out, rec))):
        tile = 128

        @pl.loop(0, data.shape[0] // tile)
        def _(i):
            at = pl.ds(pl.multiple_of(i * tile, tile), tile)
            coded[at] = jnp.dot(data[at], basis[...], preferred_element_type=F32).astype(BF16)

        for c in range(lanes):
            at = slice(c * width, (c + 1) * width)
            term[:, at] = lax.dot_general(
                coded[...], cot[:, at], (((0,), (0,)), ((), ())), preferred_element_type=F32
            )
        for k in range(nf):
            part[t * 2 + k % 2, k // 2] = term[k * span : (k + 1) * span]

    def pair_sum(t):
        return pltpu.make_async_remote_copy(
            src_ref=part.at[t * 2 + 1 - core],
            dst_ref=peer.at[t],
            send_sem=pair_sem.at[3, 0, t, 0, 0],
            recv_sem=pair_sem.at[3, 1, t, 0, 0],
            device_id=partner,
            device_id_type=MESH,
        )

    for t in range(2):
        pair_sum(t).start()
    for t in range(2):
        pair_sum(t).wait_recv()

    def ring_add(t, s, c):
        at = pl.ds(c * width, width)
        return pltpu.make_async_remote_copy(
            src_ref=hop.at[t, s, :, at],
            dst_ref=hop.at[t, s + 1, :, at],
            send_sem=send_sem.at[3, t, s, c],
            recv_sem=ring_b.at[t, s, c],
            device_id=ahead[t],
            device_id_type=MESH,
        )

    both = [(t, c) for c in range(lanes) for t in range(2)]

    def mine(t, s, c):
        position = mod(me - ways[t] * (s + 1), n)
        at = pl.ds(c * width, width)
        place = chip_at(position)
        return part[t * 2 + core, place, :, at] + peer[t, place, :, at]

    def add_stage(s):
        for t, c in both:
            at = pl.ds(c * width, width)
            ring_add(t, s - 1, c).wait_recv()
            hop[t, s, :, at] = hop[t, s, :, at] + mine(t, s, c)
            ring_add(t, s, c).start()

    for t, c in both:
        at = pl.ds(c * width, width)
        hop[t, 0, :, at] = mine(t, 0, c)
        ring_add(t, 0, c).start()
    loop(1, n - 1, add_stage)
    for t, c in both:
        at = pl.ds(c * width, width)
        ring_add(t, n - 2, c).wait_recv()
        hop[t, n - 1, :, at] = hop[t, n - 1, :, at] + mine(t, n - 1, c)

    low = [hop[t, n - 1] for t in range(2)]
    square = jnp.sum(low[0] * low[0] + low[1] * low[1], axis=(0, 1), keepdims=True)
    tots[my_id] = jnp.broadcast_to(square, tots.shape[1:])

    def tell(i):
        return pltpu.make_async_remote_copy(
            src_ref=tots.at[my_id],
            dst_ref=tots.at[my_id],
            send_sem=tot_sem.at[0],
            recv_sem=tot_sem.at[1],
            device_id=other(i),
            device_id_type=MESH,
        )

    @pl.loop(1, everyone)
    def _(i):
        tell(i).start()

    def sent_adds(s):
        for t, c in both:
            ring_add(t, s, c).wait_send()

    loop(0, n - 1, sent_adds)
    for t in range(2):
        pair_sum(t).wait_send()
    all_tots = tots.at[pl.ds(0, everyone - 1)]
    pltpu.make_async_copy(all_tots, all_tots, tot_sem.at[1]).wait()
    pltpu.make_async_copy(all_tots, all_tots, tot_sem.at[0]).wait()

    total = jnp.sum(tots[...], axis=0)
    clip = jnp.minimum(1.0, jnp.sqrt(F32(limit)) * lax.rsqrt(total + 1e-06))[0:1, 0:1]
    for t, (m, s2, mn, sn) in enumerate(
        ((m_in, s_in, mn_in, sn_in), (m_out, s_out, mn_out, sn_out))
    ):
        grad = clip * hop[t, n - 1]
        moment = 0.8 * m[...] + 0.2 * grad
        second = 0.9 * s2[...] + 0.1 * grad * grad
        mn[...] = moment
        sn[...] = second
        step[t, f] = moment / (jnp.sqrt(second) + 1e-08)

    gather(
        lambda t, dev, c: step.at[t, dev, :, pl.ds(c * width, width)], lanes, ring_d, 1
    )

    for t, (basis, w, wn, wb) in enumerate(
        ((bas_in, w_in, wn_in, wb_in), (bas_out, w_out, wn_out, wb_out))
    ):
        for k in range(nf):
            flat[k * span : (k + 1) * span] = step[t, k]
        whole = flat[...]
        high = whole.astype(BF16)
        rest = (whole - high.astype(F32)).astype(BF16)
        mat = own(basis, f)[...]
        update = jnp.dot(mat, rest, preferred_element_type=F32) + jnp.dot(
            mat, high, preferred_element_type=F32
        )
        new = w[...] - 0.01 * update
        wn[...] = new
        wb[...] = new.astype(BF16)

    puts = [
        pltpu.make_async_copy(wb_in, own(copy_in, f), base_sem.at[0]),
        pltpu.make_async_copy(wb_out, own(copy_out, f), base_sem.at[1]),
    ]
    for copy in puts:
        copy.start()
    for copy in puts:
        copy.wait()
    gather(lambda t, dev, c: rows((copy_in, copy_out)[t], dev, c), cut, ring_f, 2)


def body(
    saved_input,
    output_cotangent,
    recurrent_output,
    forget_logit,
    forget_cotangent,
    lower_bound,
    basis_in,
    basis_out,
    moment_in,
    second_in,
    moment_out,
    second_out,
    weight_in,
    weight_out,
):
    nf, nt = lax.axis_size("fs"), lax.axis_size("tp")
    n = nf // 2
    tokens, model = saved_input.shape
    units = recurrent_output.shape[1]
    depth, rank = basis_in.shape
    span = moment_in.shape[0]
    limit = 2.0 * rank * units * nt
    small = jax.ShapeDtypeStruct((span, units), F32)
    weight = jax.ShapeDtypeStruct((depth, units), F32)
    copied = jax.ShapeDtypeStruct((model, units), BF16)
    cut = 2 if depth % 32 == 0 else 1
    lanes = 2 if units % 256 == 0 else 1
    most = max(cut, lanes)
    hbm = pl.BlockSpec(memory_space=pl.ANY)
    vmem = pl.BlockSpec(memory_space=pltpu.VMEM)
    dma = pltpu.SemaphoreType.DMA
    outs = pl.pallas_call(
        functools.partial(kernel, nf, nt, limit),
        out_shape=(small, small, small, small, weight, weight, copied, copied),
        in_specs=[hbm] * 5 + [vmem] + [hbm] * 2 + [vmem] * 6,
        out_specs=[vmem] * 6 + [hbm] * 2,
        scratch_shapes=[
            pltpu.VMEM((tokens, model), BF16),
            pltpu.VMEM((tokens, model), BF16),
            pltpu.VMEM((tokens, units), BF16),
            pltpu.VMEM((tokens, units), BF16),
            pltpu.VMEM((tokens, units), BF16),
            pltpu.VMEM((model, rank), BF16),
            pltpu.VMEM((model, rank), BF16),
            pltpu.VMEM((tokens, units), BF16),
            pltpu.VMEM((rank, units), F32),
            pltpu.VMEM((tokens, rank), BF16),
            pltpu.VMEM((4, n, span, units), F32),
            pltpu.VMEM((2, n, span, units), F32),
            pltpu.VMEM((2, n, span, units), F32),
            pltpu.VMEM((2, nf, span, units), F32),
            pltpu.VMEM((rank, units), F32),
            pltpu.VMEM((depth, units), BF16),
            pltpu.VMEM((depth, units), BF16),
            pltpu.VMEM((nf * nt, 8, 128), F32),
            dma((5,)),
            dma((2,)),
            dma((4, 2, n - 1, most)),
            dma((2, n - 1, cut)),
            dma((2, n - 1, lanes)),
            dma((2, n - 1, lanes)),
            dma((2, n - 1, cut)),
            dma((4, 2, 2, n, most)),
            dma((2,)),
        ],
        compiler_params=pltpu.CompilerParams(
            collective_id=0, has_side_effects=True, vmem_limit_bytes=60 * 1024 * 1024
        ),
    )(
        saved_input,
        output_cotangent,
        recurrent_output,
        forget_logit,
        forget_cotangent,
        lower_bound[None, :],
        basis_in,
        basis_out,
        moment_in,
        second_in,
        moment_out,
        second_out,
        weight_in,
        weight_out.T,
    )
    return outs[:5] + (outs[5].T, outs[6], outs[7].T)


def solution(mesh):
    return jax.shard_map(
        body,
        mesh=mesh,
        in_specs=(
            P("fs", None),
            P("fs", None),
            P("fs", "tp"),
            P("fs", "tp"),
            P("fs", "tp"),
            P("tp"),
            P("fs", None),
            P("fs", None),
            P("fs", "tp"),
            P("fs", "tp"),
            P("fs", "tp"),
            P("fs", "tp"),
            P("fs", "tp"),
            P("tp", "fs"),
        ),
        out_specs=(
            P("fs", "tp"),
            P("fs", "tp"),
            P("fs", "tp"),
            P("fs", "tp"),
            P("fs", "tp"),
            P("tp", "fs"),
            P(None, "tp"),
            P("tp", None),
        ),
        check_vma=False,
    )
```

time: 378 us -> 171 us (0.45)
  waiting for transfers between devices: 284 us -> 0 us
  Pallas kernels: 0 us -> 153 us
  blocking collectives: 40 us -> 0 us
  matrix products: 17.7 us -> 0 us
  between operations: 14.9 us -> 0.7 us
  other arithmetic: 7.34 us -> 0 us
  local copies, waits for them, and re-layouts: 13.1 us -> 17 us
    all_gather x5 -> x0, waiting for transfers between devices: 221 us -> none  [the longest x1 47.8 us: body(): lax.all_gather(weight_in_new.astype(jnp.bfloat16), 'fs', axis=0, tiled=True)]
    pallas_call x0 -> x1, Pallas kernels: none -> 153 us  [body(): pl.pallas_call(functools.partial(kernel, nf, nt, limit), out_shape=(small...]
    reduce_scatter x1 -> x0, waiting for transfers between devices: 62 us -> none  [body(): lax.psum_scatter(jnp.concatenate([term_in, term_out], axis=1), 'fs', scat...]
    psum x1 -> x0, blocking collectives: 40 us -> none  [body(): total = lax.psum(jnp.sum(lowrank * lowrank), ('fs', 'tp'))]
    dot_general x4 -> x0, matrix products: 17.7 us -> none  [the longest x1 6.49 us: body(): lax.dot_general(coded_in, gate_cot, contract, preferred_element_type=jnp....]
    unnamed x12 -> x20, local copies, waits for them, and re-layouts: 11.5 us -> 15.7 us
  transfers between devices with their start and end apart: 6 -> 0, of which waited for: 6 -> 0; matrix products, arithmetic and copies ran while one was open for 5% -> 0% of each run, Pallas kernels for 0% -> 0%
where the time goes in v1:
time: 171 us
  Pallas kernels  153 us (89%)
  local copies, waits for them, and re-layouts  17 us (10%)
    pallas_call x1, Pallas kernels, body(): pl.pallas_call(functools.partial(kernel, nf, nt, limit), out_shape=(small...  153 us
    unnamed x20, local copies, waits for them, and re-layouts  15.7 us

profile of v1, /device:TPU:0, one launch (start us, length us, event | category | flops | bytes accessed | tf_op | source)
XLA Modules:
  0.0 170.8 jit_solution(16501224527323995963)
XLA Ops:
  0.6 1.3 broadcast_in_dim.3.lower_ref
  1.9 153.1 %shard_map.197 = (f32[24,768]{1,0:T(8,128)}, f32[24,768]{1,0:T(8,128)}, f32[24,768]{1,0:T(8,128)}, f32[24,768]{1,0:T(8,128)}, f32[192,768]{1,0:T(8,128)}, /*inde...) custom-call(bf16[512,3072]{1,0:T(8,128)(2,1)} %x_hbm.1, bf16[512,3072]{1,0:T(8,128)(2,1)} %y_hbm.1, ...), custom_call_target="tpu_custom_call" | custom-call | tf_op jit(solution)/shard_map/pallas_call | solution.py:387
  155.0 0.0 copy-start.5
  155.0 0.0 copy-start.4
  155.0 0.0 copy-start.3
  155.0 0.0 copy-start.2
  155.0 0.0 copy-start.1
  155.0 0.0 copy-start
  155.0 6.7 %copy.22 = bf16[768,3072]{1,0:T(8,128)(2,1)} copy(bf16[768,3072]{0,1:T(8,128)(2,1)} %bitcast.3) | data formatting | bytes 9437184
  161.7 0.0 copy-done.5
  161.7 0.6 copy.30
  162.4 0.0 copy-done.4
  162.4 0.6 copy.31
  163.0 0.0 copy-done.3
  163.0 0.6 copy.32
  163.7 0.0 copy-done.2
  163.7 0.6 copy.33
  164.3 0.0 copy-done.1
  164.3 0.8 copy.34
  165.1 0.0 copy-done
  165.1 0.8 copy.35
  165.9 4.8 %copy.36 = bf16[3072,768]{1,0:T(8,128)(2,1)} copy(bf16[3072,768]{1,0:T(8,128)(2,1)} %get-tuple-element.46) | data formatting | bytes 9437184
Async XLA Ops:
  155.0 6.8 %copy-start.5 = (f32[24,768]{1,0:T(8,128)S(1)}, f32[24,768]{1,0:T(8,128)}, u32[]{:S(2)}) copy-start(f32[24,768]{1,0:T(8,128)} %get-tuple-element.40) | copy-start | bytes 221188
  155.0 7.4 %copy-start.4 = (f32[24,768]{1,0:T(8,128)S(1)}, f32[24,768]{1,0:T(8,128)}, u32[]{:S(2)}) copy-start(f32[24,768]{1,0:T(8,128)} %get-tuple-element.41) | copy-start | bytes 221188
  155.0 8.0 %copy-start.3 = (f32[24,768]{1,0:T(8,128)S(1)}, f32[24,768]{1,0:T(8,128)}, u32[]{:S(2)}) copy-start(f32[24,768]{1,0:T(8,128)} %get-tuple-element.42) | copy-start | bytes 221188
  155.0 8.7 %copy-start.2 = (f32[24,768]{1,0:T(8,128)S(1)}, f32[24,768]{1,0:T(8,128)}, u32[]{:S(2)}) copy-start(f32[24,768]{1,0:T(8,128)} %get-tuple-element.43) | copy-start | bytes 221188
  155.0 9.3 %copy-start.1 = (f32[192,768]{1,0:T(8,128)S(1)}, f32[192,768]{1,0:T(8,128)}, u32[]{:S(2)}) copy-start(f32[192,768]{1,0:T(8,128)} %get-tuple-element.44) | copy-start | bytes 1769476
  155.0 10.1 %copy-start = (f32[192,768]{1,0:T(8,128)S(1)}, f32[192,768]{1,0:T(8,128)}, u32[]{:S(2)}) copy-start(f32[192,768]{1,0:T(8,128)} %get-tuple-element.21) | copy-start | bytes 1769476

commit v2 on v1

--- a/solution.py
+++ b/solution.py
@@ -80,6 +80,7 @@
     ring_d,
     ring_f,
     pair_sem,
+    sum_sem,
     tot_sem,
 ):
     f = lax.axis_index("fs")
@@ -99,9 +100,6 @@
     def dev_at(position):
         return chip_at(position) * 2 + core
 
-    ways = (1, -1)
-    ahead = tuple((dev_at(mod(me + way, n)), tp) for way in ways)
-
     loads = [
         pltpu.make_async_copy(src, dst, load_sem.at[i])
         for i, (src, dst) in enumerate(
@@ -139,55 +137,79 @@
 
     pl.semaphore_wait(barrier, everyone - 1)
 
-    def gather(view, chunks, ring_sem, phase, between=None):
-        def ring_copy(t, s, c):
-            block = view(t, dev_at(mod(me - ways[t] * s, n)), c)
+    far = n // 2
+    near = n - 1 - far
+    one_way = ((0, 1, n - 1), (1, -1, n - 1))
+    two_way = ((0, 1, far), (1, -1, far), (0, -1, near), (1, 1, near))
+
+    def neighbour(way):
+        return (dev_at(mod(me + way, n)), tp)
+
+    def gather(flows, view, chunks, ring_sem, phase, between=None):
+        stride = flows[0][2]
+
+        def remote(j, s, c, sems, target):
+            t, way, _ = flows[j]
+            block = view(t, dev_at(mod(me - way * s, n)), c)
             return pltpu.make_async_remote_copy(
                 src_ref=block,
                 dst_ref=block,
-                send_sem=send_sem.at[phase, t, s, c],
-                recv_sem=ring_sem.at[t, s, c],
-                device_id=ahead[t],
+                send_sem=sems[0],
+                recv_sem=sems[1],
+                device_id=target,
                 device_id_type=MESH,
             )
 
-        def pair_copy(t, s, c):
-            block = view(t, dev_at(mod(me - ways[t] * s, n)), c)
-            return pltpu.make_async_remote_copy(
-                src_ref=block,
-                dst_ref=block,
-                send_sem=pair_sem.at[phase, 0, t, s, c],
-                recv_sem=pair_sem.at[phase, 1, t, s, c],
-                device_id=partner,
-                device_id_type=MESH,
-            )
-
-        both = [(t, c) for c in range(chunks) for t in range(2)]
-
-        def stage(s, first=False, last=False):
-            for t, c in both:
-                if not first:
-                    ring_copy(t, s - 1, c).wait_recv()
-                if not last:
-                    ring_copy(t, s, c).start()
-                pair_copy(t, s, c).start()
-
-        stage(0, first=True)
+        def ring_copy(j, s, c):
+            sems = send_sem.at[phase, j * stride + s, c], ring_sem.at[j, s, c]
+            return remote(j, s, c, sems, neighbour(flows[j][1]))
+
+        def pair_copy(j, s, c):
+            at = j * (stride + 1) + s
+            sems = pair_sem.at[phase, 0, at, c], pair_sem.at[phase, 1, at, c]
+            return remote(j, s, c, sems, partner)
+
+        def each(s, act):
+            for c in range(chunks):
+                for j in range(len(flows)):
+                    act(j, s, c)
+
+        def move(j, s, c, first=False, last=False):
+            if not first:
+                ring_copy(j, s - 1, c).wait_recv()
+            if not last:
+                ring_copy(j, s, c).start()
+            if not first or j < 2:
+                pair_copy(j, s, c).start()
+
+        least = min(hops for _, _, hops in flows)
+        most = max(hops for _, _, hops in flows)
+        each(0, functools.partial(move, first=True))
         if between is not None:
             between()
-        loop(1, n - 1, stage)
-        stage(n - 1, last=True)
-
-        def finish(s):
-            for t, c in both:
-                pair_copy(t, s, c).wait()
-
-        def sent(s):
-            for t, c in both:
-                ring_copy(t, s, c).wait_send()
-
-        loop(0, n, finish)
-        loop(0, n - 1, sent)
+        loop(1, least, lambda s: each(s, move))
+        for s in range(least, most + 1):
+            for c in range(chunks):
+                for j, (_, _, hops) in enumerate(flows):
+                    if s <= hops:
+                        move(j, s, c, last=s == hops)
+
+        def finish(j, s, c):
+            pair_copy(j, s, c).wait()
+
+        def sent(j, s, c):
+            ring_copy(j, s, c).wait_send()
+
+        for c in range(chunks):
+            for j, (_, _, hops) in enumerate(flows):
+                if j < 2:
+                    finish(j, 0, c)
+                for s in range(least, hops):
+                    sent(j, s, c)
+                for s in range(least, hops + 1):
+                    finish(j, s, c)
+        loop(1, least, lambda s: each(s, finish))
+        loop(0, least, lambda s: each(s, sent))
 
     def make_gate():
         loads[0].wait()
@@ -204,7 +226,14 @@
 
     for copy in own_loads:
         copy.wait()
-    gather(lambda t, dev, c: rows((bas_in, bas_out)[t], dev, c), cut, ring_a, 0, make_gate)
+    gather(
+        one_way,
+        lambda t, dev, c: rows((bas_in, bas_out)[t], dev, c),
+        cut,
+        ring_a,
+        0,
+        make_gate,
+    )
 
     for copy in loads[2:]:
         copy.wait()
@@ -213,7 +242,7 @@
     lanes = 2 if units % 256 == 0 else 1
     width = units // lanes
 
-    for t, (data, basis, cot) in enumerate(((x, bas_in, gate), (y, bas_out, rec))):
+    def encode(data, basis):
         tile = 128
 
         @pl.loop(0, data.shape[0] // tile)
@@ -221,6 +250,7 @@
             at = pl.ds(pl.multiple_of(i * tile, tile), tile)
             coded[at] = jnp.dot(data[at], basis[...], preferred_element_type=F32).astype(BF16)
 
+    def project(t, cot):
         for c in range(lanes):
             at = slice(c * width, (c + 1) * width)
             term[:, at] = lax.dot_general(
@@ -233,54 +263,71 @@
         return pltpu.make_async_remote_copy(
             src_ref=part.at[t * 2 + 1 - core],
             dst_ref=peer.at[t],
-            send_sem=pair_sem.at[3, 0, t, 0, 0],
-            recv_sem=pair_sem.at[3, 1, t, 0, 0],
+            send_sem=sum_sem.at[0, t],
+            recv_sem=sum_sem.at[1, t],
             device_id=partner,
             device_id_type=MESH,
         )
 
-    for t in range(2):
-        pair_sum(t).start()
-    for t in range(2):
-        pair_sum(t).wait_recv()
-
-    def ring_add(t, s, c):
+    def ring_add(j, s, c):
         at = pl.ds(c * width, width)
         return pltpu.make_async_remote_copy(
-            src_ref=hop.at[t, s, :, at],
-            dst_ref=hop.at[t, s + 1, :, at],
-            send_sem=send_sem.at[3, t, s, c],
-            recv_sem=ring_b.at[t, s, c],
-            device_id=ahead[t],
+            src_ref=hop.at[j, s, :, at],
+            dst_ref=hop.at[j, s + 1, :, at],
+            send_sem=send_sem.at[3, j * far + s, c],
+            recv_sem=ring_b.at[j, s, c],
+            device_id=neighbour(two_way[j][1]),
             device_id_type=MESH,
         )
 
-    both = [(t, c) for c in range(lanes) for t in range(2)]
-
-    def mine(t, s, c):
-        position = mod(me - ways[t] * (s + 1), n)
+    def mine(j, s, c):
+        t, way, hops = two_way[j]
         at = pl.ds(c * width, width)
-        place = chip_at(position)
+        place = chip_at(mod(me + way * (hops - s), n))
         return part[t * 2 + core, place, :, at] + peer[t, place, :, at]
 
-    def add_stage(s):
-        for t, c in both:
+    def begin(t):
+        pair_sum(t).wait_recv()
+        for c in range(lanes):
             at = pl.ds(c * width, width)
-            ring_add(t, s - 1, c).wait_recv()
-            hop[t, s, :, at] = hop[t, s, :, at] + mine(t, s, c)
-            ring_add(t, s, c).start()
-
-    for t, c in both:
+            for j in (t, t + 2):
+                if two_way[j][2] > 0:
+                    hop[j, 0, :, at] = mine(j, 0, c)
+                    ring_add(j, 0, c).start()
+
+    def relay(j, s, c):
         at = pl.ds(c * width, width)
-        hop[t, 0, :, at] = mine(t, 0, c)
-        ring_add(t, 0, c).start()
-    loop(1, n - 1, add_stage)
-    for t, c in both:
-        at = pl.ds(c * width, width)
-        ring_add(t, n - 2, c).wait_recv()
-        hop[t, n - 1, :, at] = hop[t, n - 1, :, at] + mine(t, n - 1, c)
-
-    low = [hop[t, n - 1] for t in range(2)]
+        ring_add(j, s - 1, c).wait_recv()
+        hop[j, s, :, at] = hop[j, s, :, at] + mine(j, s, c)
+        ring_add(j, s, c).start()
+
+    def flows_do(act, s, which=range(4)):
+        for c in range(lanes):
+            for j in which:
+                act(j, s, c)
+
+    encode(x, bas_in)
+    project(0, gate)
+    pair_sum(0).start()
+    encode(y, bas_out)
+    begin(0)
+    project(1, rec)
+    pair_sum(1).start()
+    begin(1)
+    loop(1, near, lambda s: flows_do(relay, s))
+    flows_do(relay, far - 1, range(2))
+    for c in range(lanes):
+        for t in range(2):
+            at = pl.ds(c * width, width)
+            ring_add(t + 2, near - 1, c).wait_recv()
+            hop[t + 2, near, :, at] = hop[t + 2, near, :, at] + mine(t + 2, near, c)
+    for c in range(lanes):
+        for t in range(2):
+            at = pl.ds(c * width, width)
+            ring_add(t, far - 1, c).wait_recv()
+            hop[t, far, :, at] = hop[t, far, :, at] + hop[t + 2, near, :, at]
+
+    low = [hop[t, far] for t in range(2)]
     square = jnp.sum(low[0] * low[0] + low[1] * low[1], axis=(0, 1), keepdims=True)
     tots[my_id] = jnp.broadcast_to(square, tots.shape[1:])
 
@@ -298,11 +345,11 @@
     def _(i):
         tell(i).start()
 
-    def sent_adds(s):
-        for t, c in both:
-            ring_add(t, s, c).wait_send()
-
-    loop(0, n - 1, sent_adds)
+    def sent_add(j, s, c):
+        ring_add(j, s, c).wait_send()
+
+    loop(0, near, lambda s: flows_do(sent_add, s))
+    flows_do(sent_add, far - 1, range(2))
     for t in range(2):
         pair_sum(t).wait_send()
     all_tots = tots.at[pl.ds(0, everyone - 1)]
@@ -314,7 +361,7 @@
     for t, (m, s2, mn, sn) in enumerate(
         ((m_in, s_in, mn_in, sn_in), (m_out, s_out, mn_out, sn_out))
     ):
-        grad = clip * hop[t, n - 1]
+        grad = clip * hop[t, far]
         moment = 0.8 * m[...] + 0.2 * grad
         second = 0.9 * s2[...] + 0.1 * grad * grad
         mn[...] = moment
@@ -322,7 +369,11 @@
         step[t, f] = moment / (jnp.sqrt(second) + 1e-08)
 
     gather(
-        lambda t, dev, c: step.at[t, dev, :, pl.ds(c * width, width)], lanes, ring_d, 1
+        two_way,
+        lambda t, dev, c: step.at[t, dev, :, pl.ds(c * width, width)],
+        lanes,
+        ring_d,
+        1,
     )
 
     for t, (basis, w, wn, wb) in enumerate(
@@ -349,7 +400,21 @@
         copy.start()
     for copy in puts:
         copy.wait()
-    gather(lambda t, dev, c: rows((copy_in, copy_out)[t], dev, c), cut, ring_f, 2)
+    gather(
+        one_way, lambda t, dev, c: rows((copy_in, copy_out)[t], dev, c), cut, ring_f, 2
+    )
+
+
+def settle(*refs):
+    ins, outs = refs[:8], refs[8:]
+
+    @pl.when(pl.program_id(0) == 0)
+    def _():
+        for src, dst in zip(ins[:6], outs[:6]):
+            dst[...] = src[...]
+
+    outs[6][...] = ins[6][...]
+    outs[7][...] = ins[7][...].T
 
 
 def body(
@@ -402,7 +467,7 @@
             pltpu.VMEM((tokens, rank), BF16),
             pltpu.VMEM((4, n, span, units), F32),
             pltpu.VMEM((2, n, span, units), F32),
-            pltpu.VMEM((2, n, span, units), F32),
+            pltpu.VMEM((4, n // 2 + 1, span, units), F32),
             pltpu.VMEM((2, nf, span, units), F32),
             pltpu.VMEM((rank, units), F32),
             pltpu.VMEM((depth, units), BF16),
@@ -410,12 +475,13 @@
             pltpu.VMEM((nf * nt, 8, 128), F32),
             dma((5,)),
             dma((2,)),
-            dma((4, 2, n - 1, most)),
+            dma((4, 2 * n, most)),
             dma((2, n - 1, cut)),
-            dma((2, n - 1, lanes)),
-            dma((2, n - 1, lanes)),
+            dma((4, n // 2, lanes)),
+            dma((4, n // 2 + 1, lanes)),
             dma((2, n - 1, cut)),
-            dma((4, 2, 2, n, most)),
+            dma((3, 2, 2 * n + 4, most)),
+            dma((2, 2)),
             dma((2,)),
         ],
         compiler_params=pltpu.CompilerParams(
@@ -437,7 +503,20 @@
         weight_in,
         weight_out.T,
     )
-    return outs[:5] + (outs[5].T, outs[6], outs[7].T)
+    blocks = 8 if model % 1024 == 0 else 1
+    rows = model // blocks
+    tall = pl.BlockSpec((rows, units), lambda i: (i, 0))
+    kept = [pl.BlockSpec(o.shape, lambda i: (0, 0)) for o in outs[:6]]
+    outs = pl.pallas_call(
+        settle,
+        grid=(blocks,),
+        out_shape=(small, small, small, small, weight, weight, copied)
+        + (jax.ShapeDtypeStruct((units, model), BF16),),
+        in_specs=kept + [tall, tall],
+        out_specs=kept + [tall, pl.BlockSpec((units, rows), lambda i: (0, i))],
+        compiler_params=pltpu.CompilerParams(dimension_semantics=("arbitrary",)),
+    )(*outs)
+    return tuple(outs[:5]) + (outs[5].T, outs[6], outs[7])
 
 
 def solution(mesh):

time: 171 us -> 150 us (0.88)
  local copies, waits for them, and re-layouts: 17 us -> 1.27 us
  Pallas kernels: 153 us -> 147 us
    pallas_call x1, Pallas kernels: 153 us -> 137 us  [body(): pl.pallas_call(functools.partial(kernel, nf, nt, limit), out_shape=(small...]
    unnamed x20 -> x0, local copies, waits for them, and re-layouts: 15.7 us -> none
    pallas_call x0 -> x1, Pallas kernels: none -> 10.9 us  [body(): pl.pallas_call(settle, grid=(blocks,), out_shape=(small, small, small, sm...]
where the time goes in v2:
time: 150 us; the launch traced here: 149 us
  Pallas kernels  147 us (98%)
    pallas_call x1, Pallas kernels, body(): pl.pallas_call(functools.partial(kernel, nf, nt, limit), out_shape=(small...  137 us
    pallas_call x1, Pallas kernels, body(): pl.pallas_call(settle, grid=(blocks,), out_shape=(small, small, small, sm...  10.9 us

profile of v2, /device:TPU:0, one launch (start us, length us, event | category | flops | bytes accessed | tf_op | source)
XLA Modules:
  0.0 149.3 jit_solution(5309802499981705465)
XLA Ops:
  0.6 1.3 broadcast_in_dim.3.lower_ref
  1.9 136.5 %shard_map.197 = (f32[24,768]{1,0:T(8,128)}, f32[24,768]{1,0:T(8,128)}, f32[24,768]{1,0:T(8,128)}, f32[24,768]{1,0:T(8,128)}, f32[192,768]{1,0:T(8,128)}, /*inde...) custom-call(bf16[512,3072]{1,0:T(8,128)(2,1)} %x_hbm.1, bf16[512,3072]{1,0:T(8,128)(2,1)} %y_hbm.1, ...), custom_call_target="tpu_custom_call" | custom-call | tf_op jit(solution)/shard_map/pallas_call | solution.py:452
  138.4 10.9 %shard_map.198 = (f32[24,768]{1,0:T(8,128)}, f32[24,768]{1,0:T(8,128)}, f32[24,768]{1,0:T(8,128)}, f32[24,768]{1,0:T(8,128)}, f32[192,768]{1,0:T(8,128)}, /*inde...) custom-call(f32[24,768]{1,0:T(8,128)} %get-tuple-element.24.refs_0_, ...), custom_call_target="tpu_custom_call" | custom-call | tf_op jit(solution)/shard_map/pallas_call | solution.py:510
